TPU v7x, 32 devices: a whole 2x2x4 slice. The times are simulated.
32 devices in a mesh: sp: 16 (over z, y, x), tp: 2 (over core).
Axes of the slice: x: 2, y: 2, z: 4, core: 2. Of those that a mesh axis runs over, the one named last changes fastest.
Arguments:
- stream: bfloat16 [2048, 2048], P('sp', 'tp'), may hold values from -14 to 14
- queries: bfloat16 [2048, 2048], P('sp', 'tp'), may hold values from -6 to 6
- key_rows: bfloat16 [2048, 2048], P('sp', 'tp'), may hold values from -6 to 6
- values: bfloat16 [2048, 2048], P('sp', 'tp'), may hold values from -6 to 6
- out_gate: bfloat16 [2048, 2048], P('sp', 'tp'), may hold values from -6 to 6
- in_gate: float32 [16, 2048], P('tp', 'sp'), may hold values from -4 to 120
- forget_gate: float32 [16, 2048], P('tp', 'sp'), may hold values from -1 to 20
- head_gain: float32 [2048], P('tp'), may hold values from 0.1 to 1.9
- w_out: bfloat16 [2048, 2048], P('tp'), may hold values from -0.30935922 to 0.30935922
- norm_gains: bfloat16 [3, 2048], P(None, 'tp'), may hold values from 0.099609375 to 1.8984375
- w_gate: bfloat16 [2048, 5632], P('sp', 'tp'), may hold values from -0.125 to 0.125
- w_up: bfloat16 [2048, 5632], P('sp', 'tp'), may hold values from -0.125 to 0.125
- w_down: bfloat16 [5632, 2048], P('tp', 'sp'), may hold values from -0.18655063 to 0.18655063
Outputs:
- result: bfloat16 [2048, 2048], P('sp', 'tp')
All inputs are finite; a program needn't handle non-finite values.
Results may differ from a plain program's by a relative error of at most 0.012.
Values may be sent and summed in bfloat16 or wider, within the bound.
No kernel may reach another device: no remote copies, remote signals or barrier semaphores. Data moves between devices by JAX's collectives and lax.ppermute only.
A program may use at most 128 MiB of HBM per device.

v0:
```python
import jax
import jax.numpy as jnp
from jax import lax
from jax.sharding import PartitionSpec as P

D = 2048
BLOCK = 128
EPS = 1e-06


def carried_in(value, axis, combine, identity):
    peers, position = (lax.axis_size(axis), lax.axis_index(axis))
    everything = jax.tree.map(lambda part: lax.all_gather(part, axis), value)
    start = jax.tree.map(
        lambda part, zero: jnp.broadcast_to(jnp.asarray(zero, part.dtype), part.shape),
        value,
        identity,
    )

    def turn(k, before):
        reached = k < position
        new = combine(before, jax.tree.map(lambda part: part[k], everything))
        return jax.tree.map(lambda a, b: jnp.where(reached, a, b), new, before)

    return lax.fori_loop(0, peers, turn, start)


def join_states(earlier, later):
    total_early, summit_early, memory_early = earlier
    total_late, summit_late, memory_late = later
    summit = jnp.maximum(total_late + summit_early, summit_late)
    scale_early = jnp.exp(total_late + summit_early - summit)
    scale_late = jnp.exp(summit_late - summit)
    memory = scale_early[:, None, None] * memory_early + scale_late[:, None, None] * memory_late
    return (total_early + total_late, summit, memory)


def cell_block(queries, key_rows, values, in_gate, forget_gate):
    highest = lax.Precision.HIGHEST
    tokens_here = queries.shape[0]
    heads_here = in_gate.shape[0]
    head_dim = queries.shape[1] // heads_here
    blocks = tokens_here // BLOCK
    key_scale = head_dim ** (-0.5)
    log_forget = jax.nn.log_sigmoid(forget_gate)
    cumulative = jnp.cumsum(log_forget, axis=1)
    total_log = cumulative[:, -1]
    toward = total_log[:, None] - cumulative + in_gate
    summit = jnp.max(toward, axis=1)
    weight_key = jnp.exp(toward - summit[:, None])
    key_scaled = key_rows.astype(jnp.float32).reshape(tokens_here, heads_here, head_dim) * key_scale
    value_float = values.astype(jnp.float32).reshape(tokens_here, heads_here, head_dim)
    weighted = key_scaled * weight_key.T[:, :, None]
    memory_dev = jnp.einsum("shd,she->hde", weighted, value_float, precision=highest)
    identity = (jnp.zeros_like(total_log), jnp.full_like(summit, -1e30), jnp.zeros_like(memory_dev))
    prior_total, prior_summit, prior_memory = carried_in(
        (total_log, summit, memory_dev), "sp", join_states, identity
    )
    start_summit = jnp.maximum(prior_total, prior_summit)
    carry_scale = jnp.exp(prior_summit - start_summit)
    start_memory = carry_scale[:, None, None] * prior_memory
    query_blocks = queries.reshape(blocks, BLOCK, heads_here, head_dim)
    key_blocks = key_rows.reshape(blocks, BLOCK, heads_here, head_dim)
    value_blocks = values.reshape(blocks, BLOCK, heads_here, head_dim)
    keyf_blocks = key_scaled.reshape(blocks, BLOCK, heads_here, head_dim)
    forget_blocks = log_forget.reshape(heads_here, blocks, BLOCK).transpose(1, 0, 2)
    input_blocks = in_gate.reshape(heads_here, blocks, BLOCK).transpose(1, 0, 2)
    causal = jnp.tril(jnp.ones((BLOCK, BLOCK), dtype=bool))

    def advance(carried, inputs):
        memory, stabil = carried
        query_blk, key_blk, value_blk, keyf_blk, forget_blk, input_blk = inputs
        cumul_blk = jnp.cumsum(forget_blk, axis=-1)
        within = jnp.where(
            causal, cumul_blk[:, :, None] - cumul_blk[:, None, :] + input_blk[:, None, :], -jnp.inf
        )
        across = cumul_blk + stabil[:, None]
        stable = jnp.maximum(across, jnp.max(within, axis=-1))
        weight_in = jnp.exp(within - stable[:, :, None])
        weight_out = jnp.exp(across - stable)
        raw_scores = (
            jnp.einsum("thd,shd->hts", query_blk, key_blk, preferred_element_type=jnp.float32)
            * key_scale
        )
        scores = raw_scores * weight_in
        probs_low = scores.astype(jnp.bfloat16)
        query_float = query_blk.astype(jnp.float32)
        output = jnp.einsum(
            "hts,shd->htd", probs_low, value_blk, preferred_element_type=jnp.float32
        )
        output = output + weight_out[:, :, None] * jnp.einsum(
            "thd,hde->hte", query_float, memory, precision=highest
        )
        last_sum = cumul_blk[:, -1]
        toward_blk = last_sum[:, None] - cumul_blk + input_blk
        stabil_new = jnp.maximum(last_sum + stabil, jnp.max(toward_blk, axis=-1))
        decay_now = jnp.exp(last_sum + stabil - stabil_new)
        weight_blk = jnp.exp(toward_blk - stabil_new[:, None])
        weighted_blk = keyf_blk * weight_blk.T[:, :, None]
        memory_new = decay_now[:, None, None] * memory + jnp.einsum(
            "shd,she->hde", weighted_blk, value_blk.astype(jnp.float32), precision=highest
        )
        return ((memory_new, stabil_new), output.transpose(1, 0, 2))

    _, outputs = lax.scan(
        advance,
        (start_memory, start_summit),
        (query_blocks, key_blocks, value_blocks, keyf_blocks, forget_blocks, input_blocks),
    )
    return outputs.reshape(tokens_here, heads_here, head_dim)


def shards(
    stream,
    queries,
    key_rows,
    values,
    out_gate,
    in_gate,
    forget_gate,
    head_gain,
    w_out,
    norm_gains,
    w_gate,
    w_up,
    w_down,
):
    tokens_here = queries.shape[0]
    cell = cell_block(queries, key_rows, values, in_gate, forget_gate)
    normed_cell = cell * lax.rsqrt(jnp.mean(cell * cell, axis=-1, keepdims=True) + EPS)
    mixed = (
        normed_cell.reshape(tokens_here, -1)
        * head_gain
        * jax.nn.sigmoid(out_gate.astype(jnp.float32))
    ).astype(jnp.bfloat16)
    partial_mix = jnp.dot(mixed, w_out, preferred_element_type=jnp.float32)
    own_gains = norm_gains.astype(jnp.float32)
    mix_sum = lax.psum_scatter(
        partial_mix.astype(jnp.bfloat16), "tp", scatter_dimension=1, tiled=True
    ).astype(jnp.float32)
    mix_squares = lax.psum(jnp.sum(mix_sum * mix_sum, axis=1), "tp")
    mix_norm = mix_sum * lax.rsqrt(mix_squares / D + EPS)[:, None] * own_gains[0]
    after_mix = (stream.astype(jnp.float32) + mix_norm).astype(jnp.bfloat16)
    kept_rows = after_mix.astype(jnp.float32)
    resid_squares = lax.psum(jnp.sum(kept_rows * kept_rows, axis=1), "tp")
    normed = (kept_rows * lax.rsqrt(resid_squares / D + EPS)[:, None] * own_gains[1]).astype(
        jnp.bfloat16
    )
    normed_all = lax.all_gather(normed, "tp", axis=1, tiled=True)
    gate_part = jnp.dot(
        normed_all,
        lax.all_gather(w_gate, "sp", axis=0, tiled=True),
        preferred_element_type=jnp.float32,
    )
    up_part = jnp.dot(
        normed_all,
        lax.all_gather(w_up, "sp", axis=0, tiled=True),
        preferred_element_type=jnp.float32,
    )
    hidden = (jax.nn.silu(gate_part) * up_part).astype(jnp.bfloat16)
    ffn_terms = jnp.dot(
        hidden, lax.all_gather(w_down, "sp", axis=1, tiled=True), preferred_element_type=jnp.float32
    )
    ffn_sum = lax.psum_scatter(
        ffn_terms.astype(jnp.bfloat16), "tp", scatter_dimension=1, tiled=True
    ).astype(jnp.float32)
    ffn_squares = lax.psum(jnp.sum(ffn_sum * ffn_sum, axis=1), "tp")
    ffn_norm = ffn_sum * lax.rsqrt(ffn_squares / D + EPS)[:, None] * own_gains[2]
    return (kept_rows + 0.5 * ffn_norm).astype(jnp.bfloat16)


def solution(mesh):
    in_specs = (
        P("sp", "tp"),
        P("sp", "tp"),
        P("sp", "tp"),
        P("sp", "tp"),
        P("sp", "tp"),
        P("tp", "sp"),
        P("tp", "sp"),
        P("tp"),
        P("tp", None),
        P(None, "tp"),
        P("sp", "tp"),
        P("sp", "tp"),
        P("tp", "sp"),
    )
    out_specs = P("sp", "tp")
    return jax.shard_map(shards, mesh=mesh, in_specs=in_specs, out_specs=out_specs, check_vma=False)
```

profile of v0, /device:TPU:0, one launch (start us, length us, event | category | flops | bytes accessed | tf_op | source)
XLA Modules:
  0.0 661.8 jit_solution(8286072181642715078)
XLA Ops:
  6.5 0.7 fusion.46
  7.8 0.9 fusion.47
  8.6 0.8 multiply_bitcast_fusion
  9.4 1.1 copy.35
  10.5 1.1 copy.36
  11.6 1.5 fusion.24
  13.3 1.2 dynamic-slice.2
  15.6 44.4 %all-reduce.2 = (f32[128]{0:T(128)S(1)}, f32[128]{0:T(128)S(1)}) all-reduce(f32[128]{0:T(128)S(1)} %dynamic-update-slice, f32[128]{0:T(128)S(1)} %dynamic-update-slice.1), channel_id=2, replica_groups=mesh['sp'=16,'tp'=2] {'sp'}, use_global_device_ids=true, to_apply=%add | all-reduce | flops 256 | bytes 2048
  60.2 1.1 fusion.27
  61.3 67.6 %all-gather.14.cloned.1.call-done = f32[128,128,128]{2,1,0:T(8,128)} async-done(((f32[8,128,128]{2,1,0:T(8,128)}), f32[128,128,128]{2,1,0:T(8,128)}) %all-gather.14.cloned.1.call-update) | async-done | bytes 8388624 | tf_op jit(solution)/shard_map/all_gather | solution.py:13
  128.8 20.3 %while.5 = (s32[]{:T(128)}, f32[8]{0:T(128)S(1)}, f32[8]{0:T(128)S(1)}, f32[8,128,128]{2,1,0:T(8,128)S(1)}, s32[]{:T(128)}, /*index=5*/f32[16,8]{1,0:T(8,128)S(1...) while((s32[]{:T(128)}, f32[8]{0:T(128)S(1)}, f32[8]{0:T(128)S(1)}, ...), condition=%wide.region_3.4_spmd.clone, body=%wide.region_2.3_spmd.clone.sunk | while | flops 655452 | bytes 1573449 | solution.py:25
  128.9 1.2 fusion.70
  130.2 1.2 fusion.70
  131.4 1.2 fusion.70
  132.7 1.2 fusion.70
  134.0 1.2 fusion.70
  135.2 1.2 fusion.70
  136.5 1.2 fusion.70
  137.8 1.2 fusion.70
  139.1 1.2 fusion.70
  140.3 1.2 fusion.70
  141.6 1.2 fusion.70
  142.9 1.2 fusion.70
  144.1 1.2 fusion.70
  145.4 1.2 fusion.70
  146.7 1.2 fusion.70
  148.0 1.2 fusion.70
  149.4 0.7 fusion.8
  150.0 0.6 multiply_reduce_fusion
  150.9 3.8 convolution_convert_fusion.1
  154.8 0.7 all-gather.8.cloned.1.call-update
  155.5 0.5 all-gather.10.cloned.1.call-update
  156.1 0.5 all-gather.12.cloned.1.call-update
  156.7 4.3 reduce-scatter.3.cloned.1.call-done
  161.0 1.1 fusion.10
  162.1 2.5 psum.21
  164.5 1.2 fusion.17
  165.8 2.5 psum.22
  168.4 2.2 all_gather.32
  170.6 135.7 %all-gather.8.cloned.1.call-done = bf16[2048,2816]{1,0:T(8,128)(2,1)} async-done(((bf16[128,2816]{1,0:T(8,128)(2,1)}), bf16[2048,2816]{1,0:T(8,128)(2,1)}) %all-gather.8.cloned.1.call-update) | async-done | bytes 11534352 | tf_op jit(solution)/shard_map/all_gather | solution.py:152
  306.3 5.9 fusion.57
  312.2 136.3 %all-gather.10.cloned.1.call-done = bf16[2048,2816]{1,0:T(8,128)(2,1)} async-done(((bf16[128,2816]{1,0:T(8,128)(2,1)}), bf16[2048,2816]{1,0:T(8,128)(2,1)}) %all-gather.10.cloned.1.call-update) | async-done | bytes 11534352 | tf_op jit(solution)/shard_map/all_gather | solution.py:157
  448.5 182.8 %all-gather.12.cloned.1.call-done = bf16[2816,2048]{1,0:T(8,128)(2,1)} async-done(((bf16[2816,128]{1,0:T(8,128)(2,1)}), bf16[2816,2048]{1,0:T(8,128)(2,1)}) %all-gather.12.cloned.1.call-update) | async-done | bytes 11534352 | tf_op jit(solution)/shard_map/all_gather | solution.py:162
  631.3 11.9 %convolution_convert_fusion = bf16[128,2048]{1,0:T(8,128)(2,1)} fusion(bf16[2816,2048]{1,0:T(8,128)(2,1)} %all-gather.12.cloned.1.call-done, bf16[128,2048]{1,0:T(8,128)(2,1)S(1)} %all_gather.32, bf16[2048,2816]{1,0:T(8,128)(2,1)} %all-gather.10.cloned.1.call-done, f32[128,2816]{1,0:T(8,128)S(1)} %fusion.57), kind=kOutput, calls=%fused_computation.16 | convolution fusion | flops 2955214848 | bytes 25559040 | tf_op jit(solution)/shard_map/dot_general | solution.py:161
  643.2 6.3 reduce-scatter.5.cloned.1.call-done
  649.5 1.1 fusion.14
  650.6 2.5 psum.23
  653.1 1.8 fusion.20
  (76 shorter events, 2.6 us)
Async XLA Ops:
  6.5 142.8 %copy-start = (bf16[128,1024]{1,0:T(8,128)(2,1)S(1)}, bf16[128,1024]{1,0:T(8,128)(2,1)}, u32[]{:S(2)}) copy-start(bf16[128,1024]{1,0:T(8,128)(2,1)} %param.16) | copy-start | bytes 786436
  6.5 122.3 %all-gather.14.cloned.1.call-start = ((), (), s32[]{:S(2)}) async-start(), calls=%async_computation.7 | async-start | bytes 8912896 | tf_op jit(solution)/shard_map/all_gather | solution.py:13
  13.2 147.8 %reduce-scatter.3.cloned.1.call-start = ((), (), s32[]{:S(2)}) async-start(), calls=%async_computation.2 | async-start | bytes 786432 | tf_op jit(solution)/shard_map/reduce_scatter | solution.py:138
  128.8 21.2 %copy-start.2 = (f32[8,128]{1,0:T(8,128)S(1)}, f32[8,128]{1,0:T(8,128)}, u32[]{:S(2)}) copy-start(f32[8,128]{1,0:T(8,128)} %param.20) | copy-start | bytes 12292
  149.2 1.7 copy-start.4
  149.2 1.7 copy-start.5
  150.9 5.8 copy-start.3
  150.9 13.6 %copy-start.1 = (bf16[128,1024]{1,0:T(8,128)(2,1)S(1)}, bf16[128,1024]{1,0:T(8,128)(2,1)}, u32[]{:S(2)}) copy-start(bf16[128,1024]{1,0:T(8,128)(2,1)} %param.15) | copy-start | bytes 786436
  154.7 151.6 %all-gather.8.cloned.1.call-start = ((), (), s32[]{:S(2)}) async-start(), calls=%async_computation.3 | async-start | bytes 12255232 | tf_op jit(solution)/shard_map/all_gather | solution.py:152
  155.5 293.1 %all-gather.10.cloned.1.call-start = ((), (), s32[]{:S(2)}) async-start(), calls=%async_computation.4 | async-start | bytes 12255232 | tf_op jit(solution)/shard_map/all_gather | solution.py:157
  156.0 475.3 %all-gather.12.cloned.1.call-start = ((), (), s32[]{:S(2)}) async-start(), calls=%async_computation.5 | async-start | bytes 12255232 | tf_op jit(solution)/shard_map/all_gather | solution.py:162
  156.6 492.9 %reduce-scatter.5.cloned.1.call-start = ((), (), s32[]{:S(2)}) async-start(), calls=%async_computation.6 | async-start | bytes 786432 | tf_op jit(solution)/shard_map/reduce_scatter | solution.py:164
Sparse Core Ops, SparseCore 0:
  13.3 115.4 all-gather.13
  154.8 6.0 reduce-scatter.2
  163.7 142.4 all-gather.7
  308.9 139.5 all-gather.9
  451.1 180.2 all-gather.11
  643.4 6.1 reduce-scatter.4
where the time goes:
time: 663 us; the launch traced here: 662 us
  waiting for transfers between devices  535 us (81%)
  blocking collectives  53.9 us (8%)
  other arithmetic  29.2 us (4%)
  matrix products  24.3 us (4%)
  between operations  14.3 us (2%)
    all_gather x1, waiting for transfers between devices, shards(): lax.all_gather(w_down, 'sp', axis=1, tiled=True)  183 us
    all_gather x1, waiting for transfers between devices, shards(): lax.all_gather(w_up, 'sp', axis=0, tiled=True)  136 us
    all_gather x1, waiting for transfers between devices, shards(): lax.all_gather(w_gate, 'sp', axis=0, tiled=True)  136 us
    all_gather x1, waiting for transfers between devices, carried_in(): everything = jax.tree.map(lambda part: lax.all_gather(part, axis), value)  67.6 us
    unnamed x1, blocking collectives  44.4 us
    select_n x16, other arithmetic, turn(): return jax.tree.map(lambda a, b: jnp.where(reached, a, b), new, before)  19.2 us
  transfers between devices with their start and end apart: 6, of which 6 were waited for; matrix products, arithmetic and copies ran while one was open for 2% of the time, Pallas kernels for 0%

commit v1 on v0

--- a/solution.py
+++ b/solution.py
@@ -149,7 +149,9 @@
     normed_all = lax.all_gather(normed, "tp", axis=1, tiled=True)
     gate_part = jnp.dot(
         normed_all,
-        lax.all_gather(w_gate, "sp", axis=0, tiled=True),
+        jnp.concatenate(
+            lax.all_to_all(jnp.stack([w_gate] * lax.axis_size("sp")), "sp", 0, 0), axis=0
+        ),
         preferred_element_type=jnp.float32,
     )
     up_part = jnp.dot(

time: 663 us -> 731 us (1.10)
  waiting for transfers between devices: 535 us -> 593 us
    all_to_all x0 -> x1, waiting for transfers between devices: none -> 255 us  [shards(): lax.all_to_all(jnp.stack([w_gate] * lax.axis_size('sp')), 'sp', 0, 0)]
    all_gather x1 -> x0, waiting for transfers between devices: 136 us -> none  [shards(): lax.all_gather(w_gate, 'sp', axis=0, tiled=True)]
    all_gather x1, waiting for transfers between devices: 136 us -> 72.3 us  [shards(): lax.all_gather(w_up, 'sp', axis=0, tiled=True)]
    all_gather x1, waiting for transfers between devices: 183 us -> 191 us  [shards(): lax.all_gather(w_down, 'sp', axis=1, tiled=True)]
  transfers between devices with their start and end apart: 6 -> 6, of which waited for: 6 -> 5; matrix products, arithmetic and copies ran while one was open for 2% -> 2% of each run, Pallas kernels for 0% -> 0%
where the time goes in v1:
time: 731 us; the launch traced here: 730 us
  waiting for transfers between devices  593 us (81%)
  blocking collectives  53.9 us (7%)
  other arithmetic  29.2 us (4%)
  matrix products  24.3 us (3%)
  between operations  14 us (2%)
  local copies, waits for them, and re-layouts  9.82 us (1%)
    all_to_all x1, waiting for transfers between devices, shards(): lax.all_to_all(jnp.stack([w_gate] * lax.axis_size('sp')), 'sp', 0, 0)  255 us
    all_gather x1, waiting for transfers between devices, shards(): lax.all_gather(w_down, 'sp', axis=1, tiled=True)  191 us
    all_gather x1, waiting for transfers between devices, shards(): lax.all_gather(w_up, 'sp', axis=0, tiled=True)  72.3 us
    all_gather x1, waiting for transfers between devices, carried_in(): everything = jax.tree.map(lambda part: lax.all_gather(part, axis), value)  67.6 us
    unnamed x1, blocking collectives  44.4 us
    select_n x16, other arithmetic, turn(): return jax.tree.map(lambda a, b: jnp.where(reached, a, b), new, before)  19.2 us
  transfers between devices with their start and end apart: 6, of which 5 were waited for; matrix products, arithmetic and copies ran while one was open for 2% of the time, Pallas kernels for 0%

profile of v1, /device:TPU:0, one launch (start us, length us, event | category | flops | bytes accessed | tf_op | source)
XLA Modules:
  0.0 730.0 jit_solution(12573361518333931886)
XLA Ops:
  6.6 0.7 fusion.46
  7.8 0.9 fusion.47
  8.7 0.8 multiply_bitcast_fusion
  9.4 1.1 copy.35
  10.6 1.1 copy.36
  11.7 1.5 fusion.24
  13.3 1.2 dynamic-slice.2
  15.7 44.4 %all-reduce.2 = (f32[128]{0:T(128)S(1)}, f32[128]{0:T(128)S(1)}) all-reduce(f32[128]{0:T(128)S(1)} %dynamic-update-slice, f32[128]{0:T(128)S(1)} %dynamic-update-slice.1), channel_id=2, replica_groups=mesh['sp'=16,'tp'=2] {'sp'}, use_global_device_ids=true, to_apply=%add | all-reduce | flops 256 | bytes 2048
  60.3 1.1 fusion.27
  61.3 67.6 %all-gather.11.cloned.1.call-done = f32[128,128,128]{2,1,0:T(8,128)} async-done(((f32[8,128,128]{2,1,0:T(8,128)}), f32[128,128,128]{2,1,0:T(8,128)}) %all-gather.11.cloned.1.call-update) | async-done | bytes 8388624 | tf_op jit(solution)/shard_map/all_gather | solution.py:13
  128.9 20.3 %while.5 = (s32[]{:T(128)}, f32[8]{0:T(128)S(1)}, f32[8]{0:T(128)S(1)}, f32[8,128,128]{2,1,0:T(8,128)S(1)}, s32[]{:T(128)}, /*index=5*/f32[16,8]{1,0:T(8,128)S(1...) while((s32[]{:T(128)}, f32[8]{0:T(128)S(1)}, f32[8]{0:T(128)S(1)}, ...), condition=%wide.region_3.4_spmd.clone, body=%wide.region_2.3_spmd.clone.sunk | while | flops 655452 | bytes 1573449 | solution.py:25
  128.9 1.2 fusion.70
  130.2 1.2 fusion.70
  131.5 1.2 fusion.70
  132.7 1.2 fusion.70
  134.0 1.2 fusion.70
  135.3 1.2 fusion.70
  136.6 1.2 fusion.70
  137.8 1.2 fusion.70
  139.1 1.2 fusion.70
  140.4 1.2 fusion.70
  141.6 1.2 fusion.70
  142.9 1.2 fusion.70
  144.2 1.2 fusion.70
  145.5 1.2 fusion.70
  146.7 1.2 fusion.70
  148.0 1.2 fusion.70
  149.4 0.7 fusion.8
  150.1 0.6 multiply_reduce_fusion
  150.9 3.7 convolution_convert_fusion.1
  154.7 0.7 all-gather.7.cloned.1.call-update
  155.4 5.3 stack.2
  160.7 5.0 all-to-all-start
  165.8 0.5 all-gather.9.cloned.1.call-update
  166.5 1.1 fusion.10
  167.5 2.5 psum.21
  170.0 1.2 fusion.17
  171.3 2.5 psum.22
  173.9 2.2 all_gather.29
  176.1 254.9 %all-to-all-done = bf16[16,128,2816]{2,1,0:T(8,128)(2,1)} async-done(((bf16[16,128,2816]{2,1,0:T(8,128)(2,1)}), bf16[16,128,2816]{2,1,0:T(8,128)(2,1)}, u32[]{:S(2)}, u32[]{:S(2)}) %all-to-all-start) | async-done | bytes 11534368 | tf_op jit(solution)/shard_map/all_to_all | solution.py:153
  430.9 6.0 fusion.57
  436.9 72.3 %all-gather.7.cloned.1.call-done = bf16[2048,2816]{1,0:T(8,128)(2,1)} async-done(((bf16[128,2816]{1,0:T(8,128)(2,1)}), bf16[2048,2816]{1,0:T(8,128)(2,1)}) %all-gather.7.cloned.1.call-update) | async-done | bytes 11534352 | tf_op jit(solution)/shard_map/all_gather | solution.py:159
  509.2 190.7 %all-gather.9.cloned.1.call-done = bf16[2816,2048]{1,0:T(8,128)(2,1)} async-done(((bf16[2816,128]{1,0:T(8,128)(2,1)}), bf16[2816,2048]{1,0:T(8,128)(2,1)}) %all-gather.9.cloned.1.call-update) | async-done | bytes 11534352 | tf_op jit(solution)/shard_map/all_gather | solution.py:164
  699.9 11.9 %convolution_convert_fusion = bf16[128,2048]{1,0:T(8,128)(2,1)} fusion(bf16[2816,2048]{1,0:T(8,128)(2,1)} %all-gather.9.cloned.1.call-done, bf16[128,2048]{1,0:T(8,128)(2,1)S(1)} %all_gather.29, bf16[2048,2816]{1,0:T(8,128)(2,1)} %all-gather.7.cloned.1.call-done, f32[128,2816]{1,0:T(8,128)S(1)} %fusion.57), kind=kOutput, calls=%fused_computation.16 | convolution fusion | flops 2955214848 | bytes 25559040 | tf_op jit(solution)/shard_map/dot_general | solution.py:163
  711.8 6.3 reduce-scatter.5.cloned.1.call-done
  718.1 1.1 fusion.14
  719.1 2.5 psum.23
  721.6 1.8 fusion.20
  (80 shorter events, 2.6 us)
Async XLA Ops:
  6.5 142.9 %copy-start = (bf16[128,1024]{1,0:T(8,128)(2,1)S(1)}, bf16[128,1024]{1,0:T(8,128)(2,1)}, u32[]{:S(2)}) copy-start(bf16[128,1024]{1,0:T(8,128)(2,1)} %param.16) | copy-start | bytes 786436
  6.5 143.5 %copy-start.4 = (f32[8,128]{1,0:T(8,128)S(1)}, f32[8,128]{1,0:T(8,128)}, u32[]{:S(2)}) copy-start(f32[8,128]{1,0:T(8,128)} %param.20) | copy-start | bytes 12292
  6.5 144.4 %copy-start.6 = (bf16[128,1024]{1,0:T(8,128)(2,1)S(1)}, bf16[128,1024]{1,0:T(8,128)(2,1)}, u32[]{:S(2)}) copy-start(bf16[128,1024]{1,0:T(8,128)(2,1)} %param.19) | copy-start | bytes 786436
  6.5 144.4 %copy-start.7 = (f32[1024]{0:T(1024)S(1)}, f32[1024]{0:T(1024)}, u32[]{:S(2)}) copy-start(f32[1024]{0:T(1024)} %param.22) | copy-start | bytes 12292
  6.5 122.3 %all-gather.11.cloned.1.call-start = ((), (), s32[]{:S(2)}) async-start(), calls=%async_computation.7 | async-start | bytes 8912896 | tf_op jit(solution)/shard_map/all_gather | solution.py:13
  13.2 153.2 %reduce-scatter.3.cloned.1.call-start = ((), (), s32[]{:S(2)}) async-start(), calls=%async_computation.3 | async-start | bytes 786432 | tf_op jit(solution)/shard_map/reduce_scatter | solution.py:138
  149.2 6.2 copy-start.2
  154.7 354.5 %all-gather.7.cloned.1.call-start = ((), (), s32[]{:S(2)}) async-start(), calls=%async_computation.4 | async-start | bytes 12255232 | tf_op jit(solution)/shard_map/all_gather | solution.py:159
  160.7 5.7 copy-start.5
  160.7 9.3 %copy-start.3 = (bf16[128,1024]{1,0:T(8,128)(2,1)S(1)}, bf16[128,1024]{1,0:T(8,128)(2,1)}, u32[]{:S(2)}) copy-start(bf16[128,1024]{1,0:T(8,128)(2,1)} %param.15) | copy-start | bytes 786436
  160.7 270.2 %all-to-all-start = ((bf16[16,128,2816]{2,1,0:T(8,128)(2,1)}), bf16[16,128,2816]{2,1,0:T(8,128)(2,1)}, u32[]{:S(2)}, u32[]{:S(2)}) async-start(bf16[16,128,2816]{2,1,0:T(8,128)(2,1)} %stack.2), calls=%async_computation.1 | async-start | bytes 23068672 | tf_op jit(solution)/shard_map/all_to_all | solution.py:153
  165.8 534.1 %all-gather.9.cloned.1.call-start = ((), (), s32[]{:S(2)}) async-start(), calls=%async_computation.5 | async-start | bytes 12255232 | tf_op jit(solution)/shard_map/all_gather | solution.py:164
  166.4 551.7 %reduce-scatter.5.cloned.1.call-start = ((), (), s32[]{:S(2)}) async-start(), calls=%async_computation.6 | async-start | bytes 786432 | tf_op jit(solution)/shard_map/reduce_scatter | solution.py:166
  430.9 292.5 %copy-start.1 = (bf16[128,1024]{1,0:T(8,128)(2,1)S(1)}, bf16[128,1024]{1,0:T(8,128)(2,1)}, u32[]{:S(2)}) copy-start(bf16[128,1024]{1,0:T(8,128)(2,1)} %param.16) | copy-start | bytes 786436
Sparse Core Ops, SparseCore 0:
  13.4 115.4 all-gather.10
  154.8 6.0 reduce-scatter.2
  163.7 345.4 all-gather.6
  511.8 188.0 all-gather.8
  711.9 6.1 reduce-scatter.4
